TPU v7x, 32 devices: a whole 2x2x4 slice. The times are simulated.
32 devices in a mesh: sp: 8 (over z, x), tp: 4 (over y, core).
Axes of the slice: x: 2, y: 2, z: 4, core: 2. Of those that a mesh axis runs over, the one named last changes fastest.
Arguments:
- cotangent: bfloat16 [1024, 2048], P('sp'), may hold values from -6 to 6
- stream: bfloat16 [1024, 2048], P('sp'), may hold values from -6 to 6
- routes: int32 [1024, 2], P('sp'), may hold values from 0 to 3, all different within a row; in each aligned block of 128 rows (0 to 127, 128 to 255, ...) at most 96 rows name the same one
- route_weights: float32 [1024, 2], P('sp'), may hold values from 0.25 to 1
- gate_weight: bfloat16 [8, 2048, 2048], P('sp', None, 'tp'), may hold values from -0.125 to 0.125
- up_weight: bfloat16 [8, 2048, 2048], P('sp', None, 'tp'), may hold values from -0.125 to 0.125
- down_weight: bfloat16 [8, 2048, 2048], P('sp', 'tp'), may hold values from -0.09375 to 0.09375
- outer_gate: bfloat16 [1024, 1024], P('sp', 'tp'), may hold values from -6 to 6
- inner_gate: bfloat16 [1024, 1024], P('sp', 'tp'), may hold values from -6 to 6
- conv_input: bfloat16 [1024, 1024], P('sp', 'tp'), may hold values from -6 to 6
- conv_taps: bfloat16 [3, 1024], P(None, 'tp'), may hold values from -1 to 1
- out_weight: bfloat16 [2048, 1024], P(None, 'tp'), may hold values from -0.1875 to 0.1875
Outputs:
- gate_grad: bfloat16 [8, 2048, 2048], P('sp', None, 'tp')
- up_grad: bfloat16 [8, 2048, 2048], P('sp', None, 'tp')
- down_grad: bfloat16 [8, 2048, 2048], P('sp', 'tp')
- out_grad: float32 [2048, 1024], P('sp', 'tp')
- outer_grad: bfloat16 [1024, 1024], P('sp', 'tp')
- inner_grad: bfloat16 [1024, 1024], P('sp', 'tp')
- input_grad: bfloat16 [1024, 1024], P('sp', 'tp')
Inputs may be any that keep to these rules, and one draw needn't show every extreme that they name: `routes`: each token names two different experts. Among the 128 tokens of one index of sp no expert is named by more than 96 tokens, a bound that some block of them reaches in every draw.
All inputs are finite; a program needn't handle non-finite values.
Results may differ from a plain program's by a relative error of at most 0.02.
Values may be sent and summed in bfloat16 or wider, within the bound.
A program may use at most 64 MiB of HBM per device.

v0:
```python
import jax
import jax.numpy as jnp
from jax import lax
from jax.sharding import PartitionSpec as P


def from_behind(block, axis, distance):
    devices = range(lax.axis_size(axis))
    route = [(i - distance, i) for i in devices if i - distance in devices]
    return lax.ppermute(block, axis, route)


def per_device(
    cotangent,
    stream,
    routes,
    route_weights,
    gate_weight,
    up_weight,
    down_weight,
    outer_gate,
    inner_gate,
    conv_input,
    conv_taps,
    out_weight,
):
    groups = lax.axis_size("sp")
    tp_count = lax.axis_size("tp")
    experts = groups // 2
    tok_rows = stream.shape[0]
    model_width = stream.shape[1]
    capacity = 3 * tok_rows // experts
    slot_total = experts * capacity
    contract_first = (((0,), (0,)), ((), ()))
    contract_last = (((1,), (1,)), ((), ()))
    flat_routes = routes.reshape(-1)
    choose = (flat_routes[:, None] == jnp.arange(experts, dtype=jnp.int32)[None, :]).astype(
        jnp.int32
    )
    before = jnp.cumsum(choose, axis=0) - choose
    slot_place = flat_routes * capacity + jnp.sum(before * choose, axis=1)
    slot_table = (jnp.arange(slot_total, dtype=jnp.int32)[:, None] == slot_place[None, :]).astype(
        jnp.float32
    )
    select = jnp.sum(slot_table.reshape(slot_total, tok_rows, 2), axis=2).astype(jnp.bfloat16)
    slot_weight = jnp.sum(slot_table * route_weights.reshape(-1)[None, :], axis=1)
    block_width = model_width // tp_count
    offset = lax.axis_index("tp") * block_width
    rows_part = lax.dynamic_slice_in_dim(stream, offset, block_width, 1)
    cot_part = lax.dynamic_slice_in_dim(cotangent, offset, block_width, 1)
    sent_rows = jnp.dot(select, rows_part, preferred_element_type=jnp.float32).astype(jnp.bfloat16)
    sent_cot = (
        jnp.dot(select, cot_part, preferred_element_type=jnp.float32) * slot_weight[:, None]
    ).astype(jnp.bfloat16)
    sent_rows = jnp.repeat(sent_rows.reshape(experts, capacity, -1), 2, axis=0)
    sent_cot = jnp.repeat(sent_cot.reshape(experts, capacity, -1), 2, axis=0)
    recv_rows, recv_cot = (
        lax.all_to_all(sent_rows, "sp", split_axis=0, concat_axis=0, tiled=True),
        lax.all_to_all(sent_cot, "sp", split_axis=0, concat_axis=0, tiled=True),
    )
    recv_rows, recv_cot = (
        lax.all_gather(recv_rows, "tp", axis=2, tiled=True),
        lax.all_gather(recv_cot, "tp", axis=2, tiled=True),
    )
    slots = groups * capacity
    routed_rows = recv_rows.reshape(slots, model_width)
    routed_cot = recv_cot.reshape(slots, model_width)
    gate_local = gate_weight[0]
    up_local = up_weight[0]
    down_local = down_weight[0]
    gate_pre = jnp.dot(routed_rows, gate_local, preferred_element_type=jnp.float32)
    up_pre = jnp.dot(routed_rows, up_local, preferred_element_type=jnp.float32)
    hidden_grad = lax.dot_general(
        routed_cot, down_local, contract_last, preferred_element_type=jnp.float32
    )
    sigma = jax.nn.sigmoid(gate_pre)
    silu_gate = gate_pre * sigma
    hidden = (silu_gate * up_pre).astype(jnp.bfloat16)
    up_delta = (hidden_grad * silu_gate).astype(jnp.bfloat16)
    gate_delta = (hidden_grad * up_pre * sigma * (1.0 + gate_pre * (1.0 - sigma))).astype(
        jnp.bfloat16
    )
    gate_grad = lax.dot_general(
        routed_rows, gate_delta, contract_first, preferred_element_type=jnp.float32
    ).astype(jnp.bfloat16)[None]
    up_grad = lax.dot_general(
        routed_rows, up_delta, contract_first, preferred_element_type=jnp.float32
    ).astype(jnp.bfloat16)[None]
    down_grad = lax.dot_general(
        hidden, routed_cot, contract_first, preferred_element_type=jnp.float32
    ).astype(jnp.bfloat16)[None]
    row_partial = lax.dot_general(
        gate_delta, gate_local, contract_last, preferred_element_type=jnp.float32
    )
    row_partial = row_partial + lax.dot_general(
        up_delta, up_local, contract_last, preferred_element_type=jnp.float32
    )
    half_sums = lax.psum_scatter(
        row_partial.astype(jnp.bfloat16), "tp", scatter_dimension=1, tiled=True
    ).astype(jnp.float32)
    block_width = half_sums.shape[1]
    half_grad = half_sums.reshape(groups, capacity, block_width).astype(jnp.bfloat16)
    returned = lax.all_to_all(half_grad, "sp", split_axis=0, concat_axis=0, tiled=True)
    returned = returned.reshape(experts, 2, capacity, block_width)
    select_three = select.reshape(experts, capacity, tok_rows)
    moe_part = jnp.einsum(
        "ecr,emcd->rd", select_three, returned, preferred_element_type=jnp.float32
    ).astype(jnp.bfloat16)
    moe_grad = lax.all_gather(moe_part, "tp", axis=1, tiled=True)
    stream_grad = (cotangent.astype(jnp.float32) + moe_grad.astype(jnp.float32)).astype(
        jnp.bfloat16
    )
    taps = conv_taps.astype(jnp.float32)
    outer_f = outer_gate.astype(jnp.float32)
    inner_f = inner_gate.astype(jnp.float32)
    input_f = conv_input.astype(jnp.float32)
    mixed = inner_f * input_f
    earlier = from_behind(mixed[-2:], "sp", 1)
    padded = jnp.concatenate([earlier, mixed], axis=0)
    conv_sum = taps[0] * padded[:-2] + taps[1] * padded[1:-1] + taps[2] * padded[2:]
    conv_out = (outer_f * conv_sum).astype(jnp.bfloat16)
    out_grad = lax.psum_scatter(
        lax.dot_general(
            stream_grad, conv_out, contract_first, preferred_element_type=jnp.float32
        ).astype(jnp.bfloat16),
        "sp",
        scatter_dimension=0,
        tiled=True,
    ).astype(jnp.float32)
    conv_grad = jnp.dot(stream_grad, out_weight, preferred_element_type=jnp.float32)
    outer_grad = (conv_grad * conv_sum).astype(jnp.bfloat16)
    scaled = conv_grad * outer_f
    later = from_behind(scaled[:2], "sp", -1)
    extended = jnp.concatenate([scaled, later], axis=0)
    mixed_grad = taps[2] * extended[:-2] + taps[1] * extended[1:-1] + taps[0] * extended[2:]
    inner_grad = (mixed_grad * input_f).astype(jnp.bfloat16)
    input_grad = (mixed_grad * inner_f).astype(jnp.bfloat16)
    return (gate_grad, up_grad, down_grad, out_grad, outer_grad, inner_grad, input_grad)


def solution(mesh):
    placed = (
        P("sp", None),
        P("sp", None),
        P("sp", None),
        P("sp", None),
        P("sp", None, "tp"),
        P("sp", None, "tp"),
        P("sp", "tp", None),
        P("sp", "tp"),
        P("sp", "tp"),
        P("sp", "tp"),
        P(None, "tp"),
        P(None, "tp"),
    )
    return jax.shard_map(
        per_device,
        mesh=mesh,
        in_specs=placed,
        out_specs=(
            P("sp", None, "tp"),
            P("sp", None, "tp"),
            P("sp", "tp", None),
            P("sp", "tp"),
            P("sp", "tp"),
            P("sp", "tp"),
            P("sp", "tp"),
        ),
        check_vma=False,
    )
```

profile of v0, /device:TPU:0, one launch (start us, length us, event | category | flops | bytes accessed | tf_op | source)
XLA Modules:
  0.0 253.2 jit_solution(881290032400397519)
XLA Ops:
  7.2 0.9 copy.37
  8.2 0.1 eq.50
  8.3 0.1 eq.46
  8.5 1.2 reduce-window.6
  9.7 0.1 slice.47
  9.8 0.1 copy.39
  9.9 0.1 copy.40
  10.0 0.1 add_bitcast_fusion
  10.1 0.1 reduce_sum.39
  10.2 0.1 copy.41
  10.3 0.7 multiply_add_fusion.1
  11.0 0.1 convert_reduce_fusion.1
  11.1 1.2 convolution_convert_fusion.4
  12.3 0.1 broadcast_in_dim.19
  12.4 27.3 %all_to_all.15 = bf16[8,96,512]{2,1,0:T(8,128)(2,1)} all-to-all(bf16[8,96,512]{2,1,0:T(8,128)(2,1)S(1)} %bitcast.73), channel_id=1, replica_groups=mesh['sp'=8,'tp'=4] {'sp'}, dimensions={0} | all-to-all | bytes 1572864 | tf_op jit(solution)/shard_map/all_to_all | solution.py:58
  39.8 0.1 copy.42
  39.9 0.1 mul.132
  40.1 0.1 select_reduce_fusion
  40.2 0.3 fusion.13
  40.5 0.1 broadcast_in_dim.20
  40.6 23.3 %all_to_all.16 = bf16[8,96,512]{2,1,0:T(8,128)(2,1)} all-to-all(bf16[8,96,512]{2,1,0:T(8,128)(2,1)S(1)} %bitcast.74), channel_id=1, replica_groups=mesh['sp'=8,'tp'=4] {'sp'}, dimensions={0} | all-to-all | bytes 1572864 | tf_op jit(solution)/shard_map/all_to_all | solution.py:59
  63.9 3.5 %all-gather.3.cloned.1.call-done = bf16[8,96,2048]{2,1,0:T(8,128)(2,1)} async-done(((bf16[8,96,512]{2,1,0:T(8,128)(2,1)}), bf16[8,96,2048]{2,1,0:T(8,128)(2,1)}) %all-gather.3.cloned.1.call-update) | async-done | bytes 3145744 | tf_op jit(solution)/shard_map/all_gather | solution.py:62
  67.4 5.0 %fusion.5 = f32[768,512]{1,0:T(8,128)} fusion(bf16[768,2048]{1,0:T(8,128)(2,1)} %bitcast.86, bf16[1,2048,512]{2,1,0:T(8,128)(2,1)S(1)} %copy-done), kind=kOutput, calls=%fused_computation.10 | convolution fusion | flops 1610612736 | bytes 6815744 | tf_op jit(solution)/shard_map/dot_general | solution.py:71
  72.4 2.9 %fusion.8 = f32[768,512]{1,0:T(8,128)} fusion(bf16[768,2048]{1,0:T(8,128)(2,1)S(1)} %bitcast.88, bf16[1,2048,512]{2,1,0:T(8,128)(2,1)S(1)} %copy-done.2), kind=kOutput, calls=%fused_computation.13 | convolution fusion | flops 1610612736 | bytes 6815744 | tf_op jit(solution)/shard_map/dot_general | solution.py:72
  75.3 22.2 %all-gather.5.cloned.1.call-done = bf16[8,96,2048]{2,1,0:T(8,128)(2,1)} async-done(((bf16[8,96,512]{2,1,0:T(8,128)(2,1)}), bf16[8,96,2048]{2,1,0:T(8,128)(2,1)}) %all-gather.5.cloned.1.call-update) | async-done | bytes 3145744 | tf_op jit(solution)/shard_map/all_gather | solution.py:63
  97.5 5.7 %multiply_convert_fusion.1 = (bf16[768,512]{1,0:T(8,128)(2,1)S(1)}, bf16[768,512]{1,0:T(8,128)(2,1)S(1)}) fusion(f32[768,512]{1,0:T(8,128)} %fusion.5, f32[768,512]{1,0:T(8,128)} %fusion.8, bf16[768,2048]{1,0:T(8,128)(2,1)} %bitcast.90, bf16[1,512,2048]{2,1,0:T(8,128)(2,1)} %param.18), kind=kOutput, calls=%fused_computation.19 | convolution fusion | flops 1615724544 | bytes 9961472 | tf_op jit(solution)/shard_map/dot_general | solution.py:73
  103.3 1.8 fusion.3
  105.1 0.3 copy-done.3
  105.4 3.5 %add_convert_fusion = bf16[768,2048]{1,0:T(8,128)(2,1)} fusion(f32[768,2048]{1,0:T(8,128)S(1)} %fusion.3, bf16[768,512]{1,0:T(8,128)(2,1)S(1)} %get-tuple-element.11, bf16[1,2048,512]{2,1,0:T(8,128)(2,1)S(1)} %copy-done.3), kind=kOutput, calls=%fused_computation | convolution fusion | flops 1613758464 | bytes 12320768 | tf_op jit(solution)/shard_map/dot_general | solution.py:95
  109.0 37.9 %reduce-scatter.3.cloned.1.call-done = bf16[768,512]{1,0:T(8,128)(2,1)} async-done(((bf16[768,2048]{1,0:T(8,128)(2,1)}), bf16[768,512]{1,0:T(8,128)(2,1)}) %reduce-scatter.3.cloned.1.call-update) | async-done | bytes 786448 | tf_op jit(solution)/shard_map/reduce_scatter | solution.py:98
  146.8 5.5 %all-to-all-start.2 = ((bf16[8,96,512]{2,1,0:T(8,128)(2,1)}), bf16[8,96,512]{2,1,0:T(8,128)(2,1)S(1)}, u32[]{:S(2)}, u32[]{:S(2)}) async-start(bf16[8,96,512]{2,1,0:T(8,128)(2,1)} %bitcast.78), calls=%async_computation.3 | async-start | bytes 1572864 | tf_op jit(solution)/shard_map/all_to_all | solution.py:103
  152.4 0.9 convert_multiply_fusion.1
  153.3 3.9 %collective-permute-start = (f32[2,256]{1,0:T(2,128)S(1)}, f32[2,256]{1,0:T(2,128)S(1)}, u32[]{:S(2)}, u32[]{:S(2)}) collective-permute-start(f32[2,256]{1,0:T(2,128)S(1)} %slice.49), channel_id=1, source_target_pairs={{0,4},{4,8},{8,12},{12,16},{16,20},{20,24},{24,28},{1,5},{5,9},{9,... | collective-permute-start | bytes 6152 | tf_op jit(solution)/shard_map/ppermute | solution.py:10
  157.2 15.2 %all-to-all-done.2 = bf16[8,96,512]{2,1,0:T(8,128)(2,1)S(1)} async-done(((bf16[8,96,512]{2,1,0:T(8,128)(2,1)}), bf16[8,96,512]{2,1,0:T(8,128)(2,1)S(1)}, u32[]{:S(2)}, u32[]{:S(2)}) %all-to-all-start.2) | async-done | bytes 786464 | tf_op jit(solution)/shard_map/all_to_all | solution.py:103
  172.4 0.1 convert_reduce_fusion
  172.6 0.2 fusion.14
  172.8 6.7 %all_gather.11 = bf16[128,2048]{1,0:T(8,128)(2,1)S(1)} all-gather(bf16[128,512]{1,0:T(8,128)(2,1)S(1)} %fusion.14), channel_id=1, replica_groups=mesh['sp'=8,'tp'=4] {'tp'}, dimensions={1}, use_global_device_ids=true | all-gather | bytes 655360 | tf_op jit(solution)/shard_map/all_gather | solution.py:109
  179.5 1.0 multiply_convert_fusion.4
  180.5 1.5 convolution_convert_fusion.3
  182.1 5.2 %fusion = bf16[1,2048,512]{2,1,0:T(8,128)(2,1)} fusion(bf16[768,2048]{1,0:T(8,128)(2,1)} %bitcast.87, bf16[768,512]{1,0:T(8,128)(2,1)S(1)} %copy-done.8), kind=kOutput, calls=%fused_computation.4 | convolution fusion | flops 1611661312 | bytes 6029312 | tf_op jit(solution)/shard_map/dot_general | solution.py:83
  187.3 3.3 %fusion.2 = bf16[1,512,2048]{2,1,0:T(8,128)(2,1)} fusion(bf16[768,2048]{1,0:T(8,128)(2,1)S(1)} %bitcast.91, f32[768,512]{1,0:T(8,128)S(1)} %copy-done.21, f32[768,512]{1,0:T(8,128)S(1)} %copy-done.20), kind=kOutput, calls=%fused_computation.6 | convolution fusion | flops 1614020608 | bytes 8388608 | tf_op jit(solution)/shard_map/dot_general | solution.py:89
  190.6 1.4 collective-permute-start.1
  192.1 3.2 %fusion.1 = bf16[1,2048,512]{2,1,0:T(8,128)(2,1)} fusion(bf16[768,2048]{1,0:T(8,128)(2,1)S(1)} %bitcast.89, bf16[768,512]{1,0:T(8,128)(2,1)S(1)} %copy-done.6), kind=kOutput, calls=%fused_computation.5 | convolution fusion | flops 1611661312 | bytes 6029312 | tf_op jit(solution)/shard_map/dot_general | solution.py:86
  195.3 1.0 collective-permute-done.1
  196.2 0.7 fusion.26
  196.9 0.6 fusion.27
  197.6 47.4 %reduce-scatter.5.cloned.1.call-done = bf16[256,256]{1,0:T(8,128)(2,1)} async-done(((bf16[2048,256]{1,0:T(8,128)(2,1)}), bf16[256,256]{1,0:T(8,128)(2,1)}) %reduce-scatter.5.cloned.1.call-update) | async-done | bytes 131088 | tf_op jit(solution)/shard_map/reduce_scatter | solution.py:122
  245.0 1.6 convert_element_type.125
  (60 shorter events, 0.4 us)
Async XLA Ops:
  7.2 60.3 %copy-start = (bf16[1,2048,512]{2,1,0:T(8,128)(2,1)S(1)}, bf16[1,2048,512]{2,1,0:T(8,128)(2,1)}, u32[]{:S(2)}) copy-start(bf16[1,2048,512]{2,1,0:T(8,128)(2,1)} %param.16) | copy-start | bytes 6291460
  7.2 60.3 %all-gather.3.cloned.1.call-start = ((), (), s32[]{:S(2)}) async-start(), calls=%async_computation.5 | async-start | bytes 3932160 | tf_op jit(solution)/shard_map/all_gather | solution.py:62
  11.1 28.7 %copy-start.16 = (f32[128,2]{0,1:T(2,128)S(1)}, f32[128,2]{0,1:T(2,128)}, u32[]{:S(2)}) copy-start(f32[128,2]{0,1:T(2,128)} %param.15) | copy-start | bytes 3076
  11.1 29.1 %copy-start.1 = (bf16[128,2048]{1,0:T(8,128)(2,1)S(1)}, bf16[128,2048]{1,0:T(8,128)(2,1)}, u32[]{:S(2)}) copy-start(bf16[128,2048]{1,0:T(8,128)(2,1)} %param.12) | copy-start | bytes 1572868
  39.7 57.8 %all-gather.5.cloned.1.call-start = ((), (), s32[]{:S(2)}) async-start(), calls=%async_computation.6 | async-start | bytes 3932160 | tf_op jit(solution)/shard_map/all_gather | solution.py:63
  63.9 83.0 %reduce-scatter.3.cloned.1.call-start = ((), (), s32[]{:S(2)}) async-start(), calls=%async_computation.7 | async-start | bytes 3932160 | tf_op jit(solution)/shard_map/reduce_scatter | solution.py:98
  67.4 5.0 %copy-start.2 = (bf16[1,2048,512]{2,1,0:T(8,128)(2,1)S(1)}, bf16[1,2048,512]{2,1,0:T(8,128)(2,1)}, u32[]{:S(2)}) copy-start(bf16[1,2048,512]{2,1,0:T(8,128)(2,1)} %param.17) | copy-start | bytes 6291460
  67.4 5.0 %copy-start.17 = (bf16[8,96,2048]{2,1,0:T(8,128)(2,1)S(1)}, bf16[8,96,2048]{2,1,0:T(8,128)(2,1)}, u32[]{:S(2)}) copy-start(bf16[8,96,2048]{2,1,0:T(8,128)(2,1)} %all-gather.3.cloned.1.call-done) | copy-start | bytes 9437188
  103.2 1.9 copy-start.7
  103.2 1.9 copy-start.5
  103.3 2.2 copy-start.3
  108.9 48.3 %copy-start.15 = (bf16[3,256]{1,0:T(4,128)(2,1)S(1)}, bf16[3,256]{1,0:T(4,128)(2,1)}, u32[]{:S(2)}) copy-start(bf16[3,256]{1,0:T(4,128)(2,1)} %param.22) | copy-start | bytes 4612
  146.8 25.6 %all-to-all-start.2 = ((bf16[8,96,512]{2,1,0:T(8,128)(2,1)}), bf16[8,96,512]{2,1,0:T(8,128)(2,1)S(1)}, u32[]{:S(2)}, u32[]{:S(2)}) async-start(bf16[8,96,512]{2,1,0:T(8,128)(2,1)} %bitcast.78), calls=%async_computation.3 | async-start | bytes 1572864 | tf_op jit(solution)/shard_map/all_to_all | solution.py:103
  152.4 92.7 %reduce-scatter.5.cloned.1.call-start = ((), (), s32[]{:S(2)}) async-start(), calls=%async_computation.8 | async-start | bytes 1179648 | tf_op jit(solution)/shard_map/reduce_scatter | solution.py:122
  153.3 3.9 %copy-start.10 = (f32[128,256]{1,0:T(8,128)}, f32[128,256]{1,0:T(8,128)S(1)}, u32[]{:S(2)}) copy-start(f32[128,256]{1,0:T(8,128)S(1)} %convert_multiply_fusion.1) | copy-start | bytes 393220
  153.3 26.2 %collective-permute-start = (f32[2,256]{1,0:T(2,128)S(1)}, f32[2,256]{1,0:T(2,128)S(1)}, u32[]{:S(2)}, u32[]{:S(2)}) collective-permute-start(f32[2,256]{1,0:T(2,128)S(1)} %slice.49), channel_id=1, source_target_pairs={{0,4},{4,8},{8,12},{12,16},{16,20},{20,24},{24,28},{1,5},{5,9},{9,... | collective-permute-start | bytes 6152 | tf_op jit(solution)/shard_map/ppermute | solution.py:10
  172.4 7.1 %copy-start.4 = (bf16[2048,256]{1,0:T(8,128)(2,1)S(1)}, bf16[2048,256]{1,0:T(8,128)(2,1)}, u32[]{:S(2)}) copy-start(bf16[2048,256]{1,0:T(8,128)(2,1)} %param.23) | copy-start | bytes 3145732
  172.4 7.1 %copy-start.11 = (f32[128,256]{1,0:T(8,128)S(1)}, f32[128,256]{1,0:T(8,128)}, u32[]{:S(2)}) copy-start(f32[128,256]{1,0:T(8,128)} %copy-done.10) | copy-start | bytes 393220
  172.4 7.1 %copy-start.12 = (bf16[128,256]{1,0:T(8,128)(2,1)S(1)}, bf16[128,256]{1,0:T(8,128)(2,1)}, u32[]{:S(2)}) copy-start(bf16[128,256]{1,0:T(8,128)(2,1)} %param.19) | copy-start | bytes 196612
  180.5 1.5 copy-start.8
  182.0 5.2 %copy-start.19 = (bf16[8,96,2048]{2,1,0:T(8,128)(2,1)S(1)}, bf16[8,96,2048]{2,1,0:T(8,128)(2,1)}, u32[]{:S(2)}) copy-start(bf16[8,96,2048]{2,1,0:T(8,128)(2,1)} %all-gather.5.cloned.1.call-done) | copy-start | bytes 9437188
  182.0 5.2 %copy-start.20 = (f32[768,512]{1,0:T(8,128)S(1)}, f32[768,512]{1,0:T(8,128)}, u32[]{:S(2)}) copy-start(f32[768,512]{1,0:T(8,128)} %fusion.5) | copy-start | bytes 4718596
  182.1 5.2 %copy-start.21 = (f32[768,512]{1,0:T(8,128)S(1)}, f32[768,512]{1,0:T(8,128)}, u32[]{:S(2)}) copy-start(f32[768,512]{1,0:T(8,128)} %fusion.8) | copy-start | bytes 4718596
  187.3 3.3 %copy-start.9 = (f32[128,256]{1,0:T(8,128)S(1)}, f32[128,256]{1,0:T(8,128)}, u32[]{:S(2)}) copy-start(f32[128,256]{1,0:T(8,128)} %get-tuple-element.13) | copy-start | bytes 393220
  187.3 4.8 %copy-start.6 = (bf16[768,512]{1,0:T(8,128)(2,1)S(1)}, bf16[768,512]{1,0:T(8,128)(2,1)}, u32[]{:S(2)}) copy-start(bf16[768,512]{1,0:T(8,128)(2,1)} %copy-done.5) | copy-start | bytes 2359300
  187.3 4.8 %copy-start.18 = (bf16[8,96,2048]{2,1,0:T(8,128)(2,1)S(1)}, bf16[8,96,2048]{2,1,0:T(8,128)(2,1)}, u32[]{:S(2)}) copy-start(bf16[8,96,2048]{2,1,0:T(8,128)(2,1)} %all-gather.3.cloned.1.call-done) | copy-start | bytes 9437188
  190.6 5.6 %copy-start.13 = (bf16[128,256]{1,0:T(8,128)(2,1)S(1)}, bf16[128,256]{1,0:T(8,128)(2,1)}, u32[]{:S(2)}) copy-start(bf16[128,256]{1,0:T(8,128)(2,1)} %param.20) | copy-start | bytes 196612
  190.6 6.3 %copy-start.14 = (bf16[128,256]{1,0:T(8,128)(2,1)S(1)}, bf16[128,256]{1,0:T(8,128)(2,1)}, u32[]{:S(2)}) copy-start(bf16[128,256]{1,0:T(8,128)(2,1)} %param.21) | copy-start | bytes 196612
  190.6 5.6 %collective-permute-start.1 = (f32[2,256]{1,0:T(2,128)S(1)}, f32[2,256]{1,0:T(2,128)S(1)}, u32[]{:S(2)}, u32[]{:S(2)}) collective-permute-start(f32[2,256]{1,0:T(2,128)S(1)} %slice.54), channel_id=1, source_target_pairs={{4,0},{8,4},{12,8},{16,12},{20,16},{24,20},{28,24},{5,1},{9,5},{13... | collective-permute-start | bytes 6152 | tf_op jit(solution)/shard_map/ppermute | solution.py:10
Sparse Core Ops, SparseCore 0:
  39.9 27.5 all-gather.2
  69.0 28.4 all-gather.4
  109.1 37.7 reduce-scatter.2
  182.1 62.8 reduce-scatter.4
where the time goes:
time: 254 us; the launch traced here: 253 us
  waiting for transfers between devices  127 us (50%)
  blocking collectives  57.3 us (23%)
  matrix products  34.8 us (14%)
  between operations  14.1 us (6%)
  starting transfers between devices  11 us (4%)
  other arithmetic  6.23 us (2%)
    reduce_scatter x1, waiting for transfers between devices, per_device(): lax.psum_scatter(lax.dot_general(stream_grad, conv_out, contract_first, p...  47.4 us
    reduce_scatter x1, waiting for transfers between devices, per_device(): lax.psum_scatter(row_partial.astype(jnp.bfloat16), 'tp', scatter_dimensio...  37.9 us
    all_to_all x1, blocking collectives, per_device(): lax.all_to_all(sent_rows, 'sp', split_axis=0, concat_axis=0, tiled=True)  27.3 us
    all_to_all x1, blocking collectives, per_device(): lax.all_to_all(sent_cot, 'sp', split_axis=0, concat_axis=0, tiled=True)  23.3 us
    all_gather x1, waiting for transfers between devices, per_device(): lax.all_gather(recv_cot, 'tp', axis=2, tiled=True)  22.2 us
    all_to_all x1, waiting for transfers between devices, per_device(): lax.all_to_all(half_grad, 'sp', split_axis=0, concat_axis=0, tiled=True)  15.2 us
    all_gather x1, blocking collectives, per_device(): moe_grad = lax.all_gather(moe_part, 'tp', axis=1, tiled=True)  6.68 us
    dot_general x1, matrix products, per_device(): lax.dot_general(routed_cot, down_local, contract_last, preferred_element_...  5.69 us
  transfers between devices with their start and end apart: 7, of which 6 were waited for; matrix products, arithmetic and copies ran while one was open for 9% of the time, Pallas kernels for 0%

commit v1 on v0

--- a/solution.py
+++ b/solution.py
@@ -60,7 +60,7 @@
     )
     recv_rows, recv_cot = (
         lax.all_gather(recv_rows, "tp", axis=2, tiled=True),
-        lax.all_gather(recv_cot, "tp", axis=2, tiled=True),
+        jnp.concatenate(lax.all_gather(recv_cot, "tp"), axis=2),
     )
     slots = groups * capacity
     routed_rows = recv_rows.reshape(slots, model_width)

time: 254 us -> 258 us (1.016)
  local copies, waits for them, and re-layouts: 2.48 us -> 10.4 us
  matrix products: 34.8 us -> 31.5 us
    reshape x0 -> x1, local copies, waits for them, and re-layouts: none -> 4.32 us  [per_device(): jnp.concatenate(lax.all_gather(recv_cot, 'tp'), axis=2)]
    unnamed x46 -> x55, local copies, waits for them, and re-layouts: 1.45 us -> 5.06 us
    dot_general x1, matrix products: 5.69 us -> 2.31 us  [per_device(): lax.dot_general(routed_cot, down_local, contract_last, preferred_element_...]
where the time goes in v1:
time: 258 us
  waiting for transfers between devices  127 us (49%)
  blocking collectives  57.3 us (22%)
  matrix products  31.5 us (12%)
  between operations  14.1 us (5%)
  starting transfers between devices  11 us (4%)
  local copies, waits for them, and re-layouts  10.4 us (4%)
  other arithmetic  6.23 us (2%)
    reduce_scatter x1, waiting for transfers between devices, per_device(): lax.psum_scatter(lax.dot_general(stream_grad, conv_out, contract_first, p...  47.4 us
    reduce_scatter x1, waiting for transfers between devices, per_device(): lax.psum_scatter(row_partial.astype(jnp.bfloat16), 'tp', scatter_dimensio...  37.9 us
    all_to_all x1, blocking collectives, per_device(): lax.all_to_all(sent_rows, 'sp', split_axis=0, concat_axis=0, tiled=True)  27.3 us
    all_to_all x1, blocking collectives, per_device(): lax.all_to_all(sent_cot, 'sp', split_axis=0, concat_axis=0, tiled=True)  23.3 us
    all_gather x1, waiting for transfers between devices, per_device(): lax.all_gather(recv_cot, 'tp')  22.2 us
    all_to_all x1, waiting for transfers between devices, per_device(): lax.all_to_all(half_grad, 'sp', split_axis=0, concat_axis=0, tiled=True)  15.2 us
    all_gather x1, blocking collectives, per_device(): moe_grad = lax.all_gather(moe_part, 'tp', axis=1, tiled=True)  6.68 us
    all_to_all x1, starting transfers between devices, per_device(): lax.all_to_all(half_grad, 'sp', split_axis=0, concat_axis=0, tiled=True)  5.51 us
  transfers between devices with their start and end apart: 7, of which 6 were waited for; matrix products, arithmetic and copies ran while one was open for 9% of the time, Pallas kernels for 0%

profile of v1, /device:TPU:0, one launch (start us, length us, event | category | flops | bytes accessed | tf_op | source)
XLA Modules:
  0.0 257.8 jit_solution(11165598272904181788)
XLA Ops:
  7.2 0.9 copy.54
  8.2 0.1 eq.50
  8.3 0.1 eq.46
  8.5 1.2 reduce-window.6
  9.7 0.1 slice.47
  9.8 0.1 copy.56
  9.9 0.1 copy.57
  10.1 0.1 reduce_sum.39
  10.3 0.7 multiply_add_fusion.1
  11.1 1.2 convolution_convert_fusion.4
  12.4 27.3 %all_to_all.15 = bf16[8,96,512]{2,1,0:T(8,128)(2,1)} all-to-all(bf16[8,96,512]{2,1,0:T(8,128)(2,1)S(1)} %bitcast.82), channel_id=1, replica_groups=mesh['sp'=8,'tp'=4] {'sp'}, dimensions={0} | all-to-all | bytes 1572864 | tf_op jit(solution)/shard_map/all_to_all | solution.py:58
  39.8 0.1 copy.59
  39.9 0.1 mul.132
  40.1 0.1 select_reduce_fusion
  40.2 0.3 fusion.13
  40.6 23.3 %all_to_all.16 = bf16[8,96,512]{2,1,0:T(8,128)(2,1)} all-to-all(bf16[8,96,512]{2,1,0:T(8,128)(2,1)S(1)} %bitcast.83), channel_id=1, replica_groups=mesh['sp'=8,'tp'=4] {'sp'}, dimensions={0} | all-to-all | bytes 1572864 | tf_op jit(solution)/shard_map/all_to_all | solution.py:59
  63.9 3.5 %all-gather.4.cloned.1.call-done = bf16[8,96,2048]{2,1,0:T(8,128)(2,1)} async-done(((bf16[8,96,512]{2,1,0:T(8,128)(2,1)}), bf16[8,96,2048]{2,1,0:T(8,128)(2,1)}) %all-gather.4.cloned.1.call-update) | async-done | bytes 3145744 | tf_op jit(solution)/shard_map/all_gather | solution.py:62
  67.4 5.0 %fusion.5 = f32[768,512]{1,0:T(8,128)} fusion(bf16[768,2048]{1,0:T(8,128)(2,1)} %bitcast.95, bf16[1,2048,512]{2,1,0:T(8,128)(2,1)S(1)} %copy-done), kind=kOutput, calls=%fused_computation.10 | convolution fusion | flops 1610612736 | bytes 6815744 | tf_op jit(solution)/shard_map/dot_general | solution.py:71
  72.4 2.9 %fusion.8 = f32[768,512]{1,0:T(8,128)} fusion(bf16[768,2048]{1,0:T(8,128)(2,1)S(1)} %bitcast.97, bf16[1,2048,512]{2,1,0:T(8,128)(2,1)S(1)} %copy-done.4), kind=kOutput, calls=%fused_computation.13 | convolution fusion | flops 1610612736 | bytes 6815744 | tf_op jit(solution)/shard_map/dot_general | solution.py:72
  75.3 22.2 %all-gather.6.cloned.1.call-done = bf16[32,96,512]{2,1,0:T(8,128)(2,1)} async-done(((bf16[8,96,512]{2,1,0:T(8,128)(2,1)}), bf16[32,96,512]{2,1,0:T(8,128)(2,1)}) %all-gather.6.cloned.1.call-update) | async-done | bytes 3145744 | tf_op jit(solution)/shard_map/all_gather | solution.py:63
  97.5 4.3 %copy.60 = bf16[8,96,4,512]{3,2,1,0:T(4,128)(2,1)S(1)} copy(bf16[8,96,4,512]{3,1,0,2:T(8,128)(2,1)} %bitcast.81) | data formatting | bytes 6291456 | tf_op jit(solution)/shard_map/reshape | solution.py:63
  101.9 1.0 copy.62
  103.0 0.5 copy-done.21
  103.5 0.5 copy-done.22
  103.9 1.6 copy-done.24
  105.5 2.3 multiply_convert_fusion.1
  107.9 1.8 fusion.3
  109.7 0.3 copy-done.5
  110.0 3.5 %add_convert_fusion = bf16[768,2048]{1,0:T(8,128)(2,1)} fusion(f32[768,2048]{1,0:T(8,128)S(1)} %fusion.3, bf16[768,512]{1,0:T(8,128)(2,1)S(1)} %get-tuple-element.11, bf16[1,2048,512]{2,1,0:T(8,128)(2,1)S(1)} %copy-done.5), kind=kOutput, calls=%fused_computation | convolution fusion | flops 1613758464 | bytes 12320768 | tf_op jit(solution)/shard_map/dot_general | solution.py:95
  113.6 37.9 %reduce-scatter.3.cloned.1.call-done = bf16[768,512]{1,0:T(8,128)(2,1)} async-done(((bf16[768,2048]{1,0:T(8,128)(2,1)}), bf16[768,512]{1,0:T(8,128)(2,1)}) %reduce-scatter.3.cloned.1.call-update) | async-done | bytes 786448 | tf_op jit(solution)/shard_map/reduce_scatter | solution.py:98
  151.5 5.5 %all-to-all-start.2 = ((bf16[8,96,512]{2,1,0:T(8,128)(2,1)}), bf16[8,96,512]{2,1,0:T(8,128)(2,1)S(1)}, u32[]{:S(2)}, u32[]{:S(2)}) async-start(bf16[8,96,512]{2,1,0:T(8,128)(2,1)} %bitcast.87), calls=%async_computation.3 | async-start | bytes 1572864 | tf_op jit(solution)/shard_map/all_to_all | solution.py:103
  157.0 0.9 convert_multiply_fusion.1
  157.9 3.9 %collective-permute-start = (f32[2,256]{1,0:T(2,128)S(1)}, f32[2,256]{1,0:T(2,128)S(1)}, u32[]{:S(2)}, u32[]{:S(2)}) collective-permute-start(f32[2,256]{1,0:T(2,128)S(1)} %slice.49), channel_id=1, source_target_pairs={{0,4},{4,8},{8,12},{12,16},{16,20},{20,24},{24,28},{1,5},{5,9},{9,... | collective-permute-start | bytes 6152 | tf_op jit(solution)/shard_map/ppermute | solution.py:10
  161.9 15.2 %all-to-all-done.2 = bf16[8,96,512]{2,1,0:T(8,128)(2,1)S(1)} async-done(((bf16[8,96,512]{2,1,0:T(8,128)(2,1)}), bf16[8,96,512]{2,1,0:T(8,128)(2,1)S(1)}, u32[]{:S(2)}, u32[]{:S(2)}) %all-to-all-start.2) | async-done | bytes 786464 | tf_op jit(solution)/shard_map/all_to_all | solution.py:103
  177.1 0.1 convert_reduce_fusion
  177.2 0.2 fusion.14
  177.4 6.7 %all_gather.15 = bf16[128,2048]{1,0:T(8,128)(2,1)S(1)} all-gather(bf16[128,512]{1,0:T(8,128)(2,1)S(1)} %fusion.14), channel_id=1, replica_groups=mesh['sp'=8,'tp'=4] {'tp'}, dimensions={1}, use_global_device_ids=true | all-gather | bytes 655360 | tf_op jit(solution)/shard_map/all_gather | solution.py:109
  184.1 1.0 multiply_convert_fusion.4
  185.1 1.5 convolution_convert_fusion.3
  186.7 5.2 %fusion = bf16[1,2048,512]{2,1,0:T(8,128)(2,1)} fusion(bf16[768,2048]{1,0:T(8,128)(2,1)} %bitcast.96, bf16[768,512]{1,0:T(8,128)(2,1)S(1)} %copy-done.10), kind=kOutput, calls=%fused_computation.4 | convolution fusion | flops 1611661312 | bytes 6029312 | tf_op jit(solution)/shard_map/dot_general | solution.py:83
  191.9 3.3 %fusion.2 = bf16[1,512,2048]{2,1,0:T(8,128)(2,1)} fusion(bf16[768,2048]{1,0:T(8,128)(2,1)S(1)} %bitcast.80, f32[768,512]{1,0:T(8,128)S(1)} %copy-done.25, f32[768,512]{1,0:T(8,128)S(1)} %copy-done.23), kind=kOutput, calls=%fused_computation.6 | convolution fusion | flops 1614020608 | bytes 8388608 | tf_op jit(solution)/shard_map/dot_general | solution.py:89
  195.3 1.4 collective-permute-start.1
  196.7 3.2 %fusion.1 = bf16[1,2048,512]{2,1,0:T(8,128)(2,1)} fusion(bf16[768,2048]{1,0:T(8,128)(2,1)S(1)} %bitcast.98, bf16[768,512]{1,0:T(8,128)(2,1)S(1)} %copy-done.8), kind=kOutput, calls=%fused_computation.5 | convolution fusion | flops 1611661312 | bytes 6029312 | tf_op jit(solution)/shard_map/dot_general | solution.py:86
  199.9 1.0 collective-permute-done.1
  200.9 0.7 fusion.26
  201.6 0.6 fusion.27
  202.2 47.4 %reduce-scatter.5.cloned.1.call-done = bf16[256,256]{1,0:T(8,128)(2,1)} async-done(((bf16[2048,256]{1,0:T(8,128)(2,1)}), bf16[256,256]{1,0:T(8,128)(2,1)}) %reduce-scatter.5.cloned.1.call-update) | async-done | bytes 131088 | tf_op jit(solution)/shard_map/reduce_scatter | solution.py:122
  249.6 1.6 convert_element_type.125
  (70 shorter events, 0.8 us)
Async XLA Ops:
  7.2 60.3 %copy-start = (bf16[1,2048,512]{2,1,0:T(8,128)(2,1)S(1)}, bf16[1,2048,512]{2,1,0:T(8,128)(2,1)}, u32[]{:S(2)}) copy-start(bf16[1,2048,512]{2,1,0:T(8,128)(2,1)} %param.16) | copy-start | bytes 6291460
  7.2 60.3 %all-gather.4.cloned.1.call-start = ((), (), s32[]{:S(2)}) async-start(), calls=%async_computation.5 | async-start | bytes 3932160 | tf_op jit(solution)/shard_map/all_gather | solution.py:62
  11.1 28.7 %copy-start.18 = (f32[128,2]{0,1:T(2,128)S(1)}, f32[128,2]{0,1:T(2,128)}, u32[]{:S(2)}) copy-start(f32[128,2]{0,1:T(2,128)} %param.15) | copy-start | bytes 3076
  11.1 29.1 %copy-start.3 = (bf16[128,2048]{1,0:T(8,128)(2,1)S(1)}, bf16[128,2048]{1,0:T(8,128)(2,1)}, u32[]{:S(2)}) copy-start(bf16[128,2048]{1,0:T(8,128)(2,1)} %param.12) | copy-start | bytes 1572868
  39.7 57.8 %all-gather.6.cloned.1.call-start = ((), (), s32[]{:S(2)}) async-start(), calls=%async_computation.8 | async-start | bytes 3932160 | tf_op jit(solution)/shard_map/all_gather | solution.py:63
  63.9 87.6 %reduce-scatter.3.cloned.1.call-start = ((), (), s32[]{:S(2)}) async-start(), calls=%async_computation.6 | async-start | bytes 3932160 | tf_op jit(solution)/shard_map/reduce_scatter | solution.py:98
  67.4 5.0 %copy-start.4 = (bf16[1,2048,512]{2,1,0:T(8,128)(2,1)S(1)}, bf16[1,2048,512]{2,1,0:T(8,128)(2,1)}, u32[]{:S(2)}) copy-start(bf16[1,2048,512]{2,1,0:T(8,128)(2,1)} %param.17) | copy-start | bytes 6291460
  67.4 5.0 %copy-start.19 = (bf16[8,96,2048]{2,1,0:T(8,128)(2,1)S(1)}, bf16[8,96,2048]{2,1,0:T(8,128)(2,1)}, u32[]{:S(2)}) copy-start(bf16[8,96,2048]{2,1,0:T(8,128)(2,1)} %all-gather.4.cloned.1.call-done) | copy-start | bytes 9437188
  101.9 1.6 copy-start.21
  101.9 2.1 copy-start.22
  101.9 3.6 %copy-start.24 = (f32[768,512]{1,0:T(8,128)S(1)}, f32[768,512]{1,0:T(8,128)}, u32[]{:S(2)}) copy-start(f32[768,512]{1,0:T(8,128)} %fusion.8) | copy-start | bytes 4718596
  102.9 4.9 %copy-start.1 = (bf16[96,8,4,512]{3,1,2,0:T(8,128)(2,1)}, bf16[96,8,4,512]{3,1,2,0:T(8,128)(2,1)S(1)}, u32[]{:S(2)}) copy-start(bf16[96,8,4,512]{3,1,2,0:T(8,128)(2,1)S(1)} %copy.62) | copy-start | bytes 9437188
  107.8 1.9 copy-start.9
  107.9 1.9 copy-start.7
  107.9 2.2 copy-start.5
  113.6 48.3 %copy-start.17 = (bf16[3,256]{1,0:T(4,128)(2,1)S(1)}, bf16[3,256]{1,0:T(4,128)(2,1)}, u32[]{:S(2)}) copy-start(bf16[3,256]{1,0:T(4,128)(2,1)} %param.22) | copy-start | bytes 4612
  151.5 25.6 %all-to-all-start.2 = ((bf16[8,96,512]{2,1,0:T(8,128)(2,1)}), bf16[8,96,512]{2,1,0:T(8,128)(2,1)S(1)}, u32[]{:S(2)}, u32[]{:S(2)}) async-start(bf16[8,96,512]{2,1,0:T(8,128)(2,1)} %bitcast.87), calls=%async_computation.3 | async-start | bytes 1572864 | tf_op jit(solution)/shard_map/all_to_all | solution.py:103
  157.0 92.7 %reduce-scatter.5.cloned.1.call-start = ((), (), s32[]{:S(2)}) async-start(), calls=%async_computation.7 | async-start | bytes 1179648 | tf_op jit(solution)/shard_map/reduce_scatter | solution.py:122
  157.9 3.9 %copy-start.12 = (f32[128,256]{1,0:T(8,128)}, f32[128,256]{1,0:T(8,128)S(1)}, u32[]{:S(2)}) copy-start(f32[128,256]{1,0:T(8,128)S(1)} %convert_multiply_fusion.1) | copy-start | bytes 393220
  157.9 26.2 %collective-permute-start = (f32[2,256]{1,0:T(2,128)S(1)}, f32[2,256]{1,0:T(2,128)S(1)}, u32[]{:S(2)}, u32[]{:S(2)}) collective-permute-start(f32[2,256]{1,0:T(2,128)S(1)} %slice.49), channel_id=1, source_target_pairs={{0,4},{4,8},{8,12},{12,16},{16,20},{20,24},{24,28},{1,5},{5,9},{9,... | collective-permute-start | bytes 6152 | tf_op jit(solution)/shard_map/ppermute | solution.py:10
  177.1 7.1 %copy-start.6 = (bf16[2048,256]{1,0:T(8,128)(2,1)S(1)}, bf16[2048,256]{1,0:T(8,128)(2,1)}, u32[]{:S(2)}) copy-start(bf16[2048,256]{1,0:T(8,128)(2,1)} %param.23) | copy-start | bytes 3145732
  177.1 7.1 %copy-start.13 = (f32[128,256]{1,0:T(8,128)S(1)}, f32[128,256]{1,0:T(8,128)}, u32[]{:S(2)}) copy-start(f32[128,256]{1,0:T(8,128)} %copy-done.12) | copy-start | bytes 393220
  177.1 7.1 %copy-start.14 = (bf16[128,256]{1,0:T(8,128)(2,1)S(1)}, bf16[128,256]{1,0:T(8,128)(2,1)}, u32[]{:S(2)}) copy-start(bf16[128,256]{1,0:T(8,128)(2,1)} %param.19) | copy-start | bytes 196612
  185.1 1.5 copy-start.10
  186.7 5.2 %copy-start.2 = (bf16[96,8,4,512]{3,1,2,0:T(8,128)(2,1)S(1)}, bf16[96,8,4,512]{3,1,2,0:T(8,128)(2,1)}, u32[]{:S(2)}) copy-start(bf16[96,8,4,512]{3,1,2,0:T(8,128)(2,1)} %copy-done.1) | copy-start | bytes 9437188
  186.7 5.2 %copy-start.23 = (f32[768,512]{1,0:T(8,128)S(1)}, f32[768,512]{1,0:T(8,128)}, u32[]{:S(2)}) copy-start(f32[768,512]{1,0:T(8,128)} %fusion.5) | copy-start | bytes 4718596
  186.7 5.2 %copy-start.25 = (f32[768,512]{1,0:T(8,128)S(1)}, f32[768,512]{1,0:T(8,128)}, u32[]{:S(2)}) copy-start(f32[768,512]{1,0:T(8,128)} %fusion.8) | copy-start | bytes 4718596
  191.9 3.3 %copy-start.11 = (f32[128,256]{1,0:T(8,128)S(1)}, f32[128,256]{1,0:T(8,128)}, u32[]{:S(2)}) copy-start(f32[128,256]{1,0:T(8,128)} %get-tuple-element.13) | copy-start | bytes 393220
  191.9 4.8 %copy-start.8 = (bf16[768,512]{1,0:T(8,128)(2,1)S(1)}, bf16[768,512]{1,0:T(8,128)(2,1)}, u32[]{:S(2)}) copy-start(bf16[768,512]{1,0:T(8,128)(2,1)} %copy-done.7) | copy-start | bytes 2359300
  191.9 4.8 %copy-start.20 = (bf16[8,96,2048]{2,1,0:T(8,128)(2,1)S(1)}, bf16[8,96,2048]{2,1,0:T(8,128)(2,1)}, u32[]{:S(2)}) copy-start(bf16[8,96,2048]{2,1,0:T(8,128)(2,1)} %all-gather.4.cloned.1.call-done) | copy-start | bytes 9437188
  195.3 5.6 %copy-start.15 = (bf16[128,256]{1,0:T(8,128)(2,1)S(1)}, bf16[128,256]{1,0:T(8,128)(2,1)}, u32[]{:S(2)}) copy-start(bf16[128,256]{1,0:T(8,128)(2,1)} %param.20) | copy-start | bytes 196612
  195.3 6.3 %copy-start.16 = (bf16[128,256]{1,0:T(8,128)(2,1)S(1)}, bf16[128,256]{1,0:T(8,128)(2,1)}, u32[]{:S(2)}) copy-start(bf16[128,256]{1,0:T(8,128)(2,1)} %param.21) | copy-start | bytes 196612
  195.3 5.6 %collective-permute-start.1 = (f32[2,256]{1,0:T(2,128)S(1)}, f32[2,256]{1,0:T(2,128)S(1)}, u32[]{:S(2)}, u32[]{:S(2)}) collective-permute-start(f32[2,256]{1,0:T(2,128)S(1)} %slice.54), channel_id=1, source_target_pairs={{4,0},{8,4},{12,8},{16,12},{20,16},{24,20},{28,24},{5,1},{9,5},{13... | collective-permute-start | bytes 6152 | tf_op jit(solution)/shard_map/ppermute | solution.py:10
Sparse Core Ops, SparseCore 0:
  39.9 27.5 all-gather.3
  69.0 28.4 all-gather.5
  113.7 37.7 reduce-scatter.2
  186.8 62.8 reduce-scatter.4
